TPU v7x, 32 devices: a whole 2x2x4 slice. The times are simulated.
32 devices in a mesh: ep: 8 (over z, core), tp: 4 (over y, x).
Axes of the slice: x: 2, y: 2, z: 4, core: 2. Of those that a mesh axis runs over, the one named last changes fastest.
Arguments:
- gate_out: bfloat16 [2048, 1024], P('ep', 'tp'), may hold values from -6 to 6
- gate_in: bfloat16 [2048, 1024], P('ep', 'tp'), may hold values from -6 to 6
- conv_values: bfloat16 [2048, 1024], P('ep', 'tp'), may hold values from -6 to 6
- conv_taps: float32 [3, 1024], P(None, 'tp'), may hold values from -3 to 3
- mixer_proj: bfloat16 [1024, 2048], P('tp'), may hold values from -0.25 to 0.25
- expert_in: bfloat16 [2048, 2048], P('ep'), may hold values from -6 to 6
- norm_gain: float32 [2048], replicated, may hold values from 0.1 to 1.9
- route_ids: int32 [2048, 2], P('ep'), may hold values from 0 to 7, all different within a row; in each aligned block of 256 rows (0 to 255, 256 to 511, ...) at most 86 rows name the same one
- route_scores: float32 [2048, 2], P('ep'), may hold values from 0.1 to 1
- gate_proj: bfloat16 [8, 2048, 4096], P('ep', None, 'tp'), may hold values from -0.125 to 0.125
- up_proj: bfloat16 [8, 2048, 4096], P('ep', None, 'tp'), may hold values from -0.125 to 0.125
- down_proj: bfloat16 [8, 4096, 2048], P('ep', 'tp'), may hold values from -0.125 to 0.125
Outputs:
- mixed: bfloat16 [2048, 2048], P('ep', 'tp')
- expert_mix: bfloat16 [2048, 2048], P('ep', 'tp')
Inputs may be any that keep to these rules, and one draw needn't show every extreme that they name: `route_ids`: each row names 2 different experts. Within each aligned block of 256 rows (the rows of one device of ep) no expert is named by more than 86 rows, and in some block an expert is named by exactly 86 rows.
All inputs are finite; a program needn't handle non-finite values.
Results may differ from a plain program's by a relative error of at most 0.015.
Values may be sent and summed in bfloat16 or wider, within the bound.
A program may use at most 64 MiB of HBM per device.

v0:
```python
import jax
import jax.numpy as jnp
from jax import lax
from jax.sharding import PartitionSpec as P


def shifted(block, axis, distance):
    devices = range(lax.axis_size(axis))
    route = [(i - distance, i) for i in devices if i - distance in devices]
    return lax.ppermute(block, axis, route)


def slot_table(route_ids, experts_total, capacity):
    pairs = route_ids.reshape(-1)
    onehot = (pairs[:, None] == jnp.arange(experts_total, dtype=jnp.int32)[None, :]).astype(
        jnp.int32
    )
    before = jnp.cumsum(onehot, axis=0) - onehot
    ranking = jnp.sum(before * onehot, axis=1)
    return (pairs * capacity + ranking).reshape(route_ids.shape)


def shards(
    gate_out,
    gate_in,
    conv_values,
    conv_taps,
    mixer_proj,
    expert_in,
    norm_gain,
    route_ids,
    route_scores,
    gate_proj,
    up_proj,
    down_proj,
):
    product = gate_in.astype(jnp.float32) * conv_values.astype(jnp.float32)
    seq_len = product.shape[0]
    tap_count = conv_taps.shape[0]
    earlier = shifted(product[seq_len - (tap_count - 1) :], "ep", 1)
    padded = jnp.concatenate([earlier, product], axis=0)
    convolved = conv_taps[0] * padded[0:seq_len]
    for offset in range(1, tap_count):
        convolved = convolved + conv_taps[offset] * padded[offset : offset + seq_len]
    branch = (gate_out.astype(jnp.float32) * convolved).astype(jnp.bfloat16)
    partial_mix = jnp.dot(branch, mixer_proj, preferred_element_type=jnp.float32)
    mixed = lax.psum_scatter(
        partial_mix.astype(jnp.bfloat16), "tp", scatter_dimension=1, tiled=True
    )
    rows_wide = expert_in.astype(jnp.float32)
    scaling = lax.rsqrt(jnp.mean(rows_wide * rows_wide, axis=1, keepdims=True) + 1e-06)
    normed = (rows_wide * scaling * norm_gain).astype(jnp.bfloat16)
    token_count = expert_in.shape[0]
    choose_count = route_ids.shape[1]
    model_width = expert_in.shape[1]
    ep_count = lax.axis_size("ep")
    local_experts = gate_proj.shape[0]
    experts_total = ep_count * local_experts
    capacity = max(
        2, (4 * token_count * choose_count + 3 * experts_total - 1) // (3 * experts_total)
    )
    slot_count = experts_total * capacity
    slots = slot_table(route_ids, experts_total, capacity)
    hits = slots[None, :, :] == jnp.arange(slot_count, dtype=jnp.int32)[:, None, None]
    dispatch = jnp.sum(hits.astype(jnp.int32), axis=2).astype(jnp.bfloat16)
    column_count = model_width // lax.axis_size("tp")
    own_columns = lax.dynamic_slice_in_dim(
        normed, lax.axis_index("tp") * column_count, column_count, 1
    )
    sent = jnp.dot(dispatch, own_columns, preferred_element_type=jnp.float32).astype(jnp.bfloat16)
    arrived = lax.all_to_all(sent, "ep", split_axis=0, concat_axis=0, tiled=True)
    piece = lax.all_gather(arrived, "tp", axis=1, tiled=True)
    grouped_piece = piece.reshape(ep_count, local_experts, capacity, piece.shape[1])
    gate_part = jnp.einsum(
        "secd,edf->secf", grouped_piece, gate_proj, preferred_element_type=jnp.float32
    )
    up_part = jnp.einsum(
        "secd,edf->secf", grouped_piece, up_proj, preferred_element_type=jnp.float32
    )
    hidden = (jax.nn.silu(gate_part) * up_part).astype(jnp.bfloat16)
    partial_out = jnp.einsum(
        "secf,efd->secd", hidden, down_proj, preferred_element_type=jnp.float32
    )
    summed = lax.psum_scatter(
        partial_out.astype(jnp.bfloat16), "tp", scatter_dimension=3, tiled=True
    )
    returned = lax.all_to_all(summed, "ep", split_axis=0, concat_axis=0, tiled=True)
    slot_rows = returned.reshape(slot_count, returned.shape[3])
    picked = jnp.take(slot_rows, slots.reshape(-1), axis=0).reshape(
        token_count, choose_count, slot_rows.shape[1]
    )
    weights = route_scores / jnp.sum(route_scores, axis=1, keepdims=True)
    expert_mix = jnp.sum(weights[:, :, None] * picked.astype(jnp.float32), axis=1).astype(
        jnp.bfloat16
    )
    return (mixed, expert_mix)


def solution(mesh):
    placed = (
        P("ep", "tp"),
        P("ep", "tp"),
        P("ep", "tp"),
        P(None, "tp"),
        P("tp", None),
        P("ep", None),
        P(),
        P("ep", None),
        P("ep", None),
        P("ep", None, "tp"),
        P("ep", None, "tp"),
        P("ep", "tp", None),
    )
    return jax.shard_map(
        shards,
        mesh=mesh,
        in_specs=placed,
        out_specs=(P("ep", "tp"), P("ep", "tp")),
        check_vma=False,
    )
```

profile of v0, /device:TPU:0, one launch (start us, length us, event | category | flops | bytes accessed | tf_op | source)
XLA Modules:
  0.0 187.0 jit_solution(16390596745611525684)
XLA Ops:
  7.2 0.0 copy-start
  7.2 0.0 copy-start.5
  7.2 0.0 copy-start.1
  7.2 0.0 all-gather.2.cloned.1.call-start
  7.2 0.9 copy.33
  8.2 0.1 eq.39
  8.3 0.1 reshape.111
  8.5 2.8 %convert_element_type.67 = f32[256,2048]{1,0:T(8,128)} convert(bf16[256,2048]{1,0:T(8,128)(2,1)} %param.17) | non-fusion elementwise | flops 524288 | bytes 3145728 | tf_op jit(solution)/shard_map/convert_element_type | solution.py:50
  11.3 0.0 copy-done.1
  11.3 0.3 multiply_reduce_fusion
  11.6 1.1 reduce-window.6
  12.8 0.2 slice_reduce_fusion
  13.0 0.1 fusion.41
  13.1 0.1 reduce_sum.51
  13.3 0.1 copy.35
  13.4 0.3 convert_reduce_fusion
  13.7 0.8 dynamic-slice
  14.4 1.5 convolution_convert_fusion.1
  15.9 0.2 all_to_all.11
  16.1 25.7 %all_to_all.17 = bf16[8,86,512]{2,1,0:T(8,128)(2,1)S(1)} all-to-all(bf16[8,86,512]{2,1,0:T(8,128)(2,1)S(1)} %all_to_all.11), channel_id=1, replica_groups=mesh['ep'=8,'tp'=4] {'ep'}, dimensions={0} | all-to-all | bytes 1409024 | tf_op jit(solution)/shard_map/all_to_all | solution.py:71
  41.8 1.1 all_to_all.13
  42.9 0.0 all-gather.2.cloned.1.call-update
  42.9 0.0 reduce-scatter.5.cloned.1.call-start
  42.9 40.0 %all-gather.2.cloned.1.call-done = bf16[688,2048]{1,0:T(8,128)(2,1)} async-done(((bf16[688,512]{1,0:T(8,128)(2,1)}), bf16[688,2048]{1,0:T(8,128)(2,1)}) %all-gather.2.cloned.1.call-update) | async-done | bytes 2818064 | tf_op jit(solution)/shard_map/all_gather | solution.py:72
  83.0 3.3 %reshape.113 = bf16[8,86,2048]{2,1,0:T(8,128)(2,1)} reshape(bf16[688,2048]{1,0:T(8,128)(2,1)} %all-gather.2.cloned.1.call-done) | data formatting | bytes 5636096 | tf_op jit(solution)/shard_map/reshape.9
  86.3 7.8 %fusion.2 = f32[8,86,1024]{2,1,0:T(8,128)} fusion(bf16[8,86,2048]{2,1,0:T(8,128)(2,1)} %reshape.113, bf16[1,2048,1024]{2,1,0:T(8,128)(2,1)} %param.22), kind=kOutput, calls=%fused_computation.3 | convolution fusion | flops 2885681152 | bytes 9830400 | tf_op jit(solution)/shard_map/secd,edf->secf/dot_general | solution.py:77
  94.1 13.0 %fusion.9 = bf16[8,1,86,2048]{3,2,0,1:T(8,128)(2,1)} fusion(bf16[1,1024,2048]{2,1,0:T(8,128)(2,1)} %param.23, f32[8,86,1024]{2,1,0:T(8,128)} %fusion.2, bf16[8,86,2048]{2,1,0:T(8,128)(2,1)} %reshape.113, bf16[1,2048,1024]{2,1,0:T(8,128)(2,1)} %param.21), kind=kOutput, calls=%fused_computation.8 | convolution fusion | flops 5776998400 | bytes 16842752 | tf_op jit(solution)/shard_map/secf,efd->secd/dot_general | solution.py:81
  107.1 0.0 reduce-scatter.5.cloned.1.call-update
  107.2 0.0 copy-start.6
  107.2 0.0 reduce-scatter.3.cloned.1.call-start
  107.2 0.8 copy-done.3
  108.0 0.1 copy-done.4
  108.1 1.6 collective-permute-start
  109.7 0.8 collective-permute-done
  110.5 1.4 convolution_convert_fusion
  112.0 0.0 reduce-scatter.3.cloned.1.call-update
  112.0 37.0 %reduce-scatter.5.cloned.1.call-done = bf16[8,1,86,512]{3,2,0,1:T(8,128)(2,1)} async-done(((bf16[8,1,86,2048]{3,2,0,1:T(8,128)(2,1)}), bf16[8,1,86,512]{3,2,0,1:T(8,128)(2,1)}) %reduce-scatter.5.cloned.1.call-update) | async-done | bytes 704528 | tf_op jit(solution)/shard_map/reduce_scatter | solution.py:84
  149.0 4.6 %all-to-all-start.1 = ((bf16[8,1,86,512]{3,2,1,0:T(8,128)(2,1)}), bf16[8,1,86,512]{3,2,1,0:T(8,128)(2,1)S(1)}, u32[]{:S(2)}, u32[]{:S(2)}) async-start(bf16[8,1,86,512]{3,2,1,0:T(8,128)(2,1)} %bitcast.82), calls=%async_computation.3 | async-start | bytes 1441792 | tf_op jit(solution)/shard_map/all_to_all | solution.py:87
  153.7 0.1 copy.38
  153.8 0.1 mul.120
  154.0 0.2 copy.36
  154.2 0.1 copy.32
  154.4 18.8 %all-to-all-done.1 = bf16[8,1,86,512]{3,2,1,0:T(8,128)(2,1)S(1)} async-done(((bf16[8,1,86,512]{3,2,1,0:T(8,128)(2,1)}), bf16[8,1,86,512]{3,2,1,0:T(8,128)(2,1)S(1)}, u32[]{:S(2)}, u32[]{:S(2)}) %all-to-all-start.1) | async-done | bytes 704544 | tf_op jit(solution)/shard_map/all_to_all | solution.py:87
  173.2 0.2 reshape.118
  173.4 2.0 %gather_fusion = bf16[512,512]{1,0:T(8,128)(2,1)S(1)} fusion(bf16[688,512]{1,0:T(8,128)(2,1)S(1)} %reshape.118, s32[1024]{0:T(1024)S(1)} %pad_clamp_fusion), kind=kCustom, calls=%fused_computation | custom fusion | bytes 1050624 | tf_op jit(solution)/shard_map/jit(_take)/gather | solution.py:89
  175.4 0.2 gather.7
  175.6 2.9 %multiply_reduce_fusion.1 = bf16[256,512]{1,0:T(8,128)(2,1)} fusion(bf16[256,2,512]{2,1,0:T(2,128)(2,1)S(1)} %gather.7, pred[256,2]{1,0:T(8,128)(4,1)S(1)} %copy.36, f32[256,2]{1,0:T(8,128)S(1)} %copy.32), kind=kLoop, calls=%fused_computation.22 | loop fusion | flops 917504 | bytes 788992 | tf_op jit(solution)/shard_map/reduce_sum | solution.py:93
  178.5 2.0 %reduce-scatter.3.cloned.1.call-done = bf16[256,512]{1,0:T(8,128)(2,1)} async-done(((bf16[256,2048]{1,0:T(8,128)(2,1)}), bf16[256,512]{1,0:T(8,128)(2,1)}) %reduce-scatter.3.cloned.1.call-update) | async-done | bytes 262160 | tf_op jit(solution)/shard_map/reduce_scatter | solution.py:47
  (22 shorter events, 0.2 us)
Async XLA Ops:
  7.2 103.4 %copy-start = (bf16[256,2048]{1,0:T(8,128)(2,1)S(1)}, bf16[256,2048]{1,0:T(8,128)(2,1)}, u32[]{:S(2)}) copy-start(bf16[256,2048]{1,0:T(8,128)(2,1)} %param.16) | copy-start | bytes 3145732
  7.2 6.2 %copy-start.5 = (s32[256,2]{0,1:T(2,128)S(1)}, s32[256,2]{0,1:T(2,128)}, u32[]{:S(2)}) copy-start(s32[256,2]{0,1:T(2,128)} %param.19) | copy-start | bytes 6148
  7.2 4.1 %copy-start.1 = (bf16[256,2048]{1,0:T(8,128)(2,1)S(1)}, bf16[256,2048]{1,0:T(8,128)(2,1)}, u32[]{:S(2)}) copy-start(bf16[256,2048]{1,0:T(8,128)(2,1)} %param.17) | copy-start | bytes 3145732
  7.2 75.8 %all-gather.2.cloned.1.call-start = ((), (), s32[]{:S(2)}) async-start(), calls=%async_computation.5 | async-start | bytes 3522560 | tf_op jit(solution)/shard_map/all_gather | solution.py:72
  42.9 106.2 %reduce-scatter.5.cloned.1.call-start = ((), (), s32[]{:S(2)}) async-start(), calls=%async_computation.6 | async-start | bytes 3604480 | tf_op jit(solution)/shard_map/reduce_scatter | solution.py:84
  107.1 0.9 copy-start.3
  107.1 1.0 copy-start.4
  107.1 2.6 %copy-start.7 = (f32[3,256]{1,0:T(4,128)S(1)}, f32[3,256]{1,0:T(4,128)}, u32[]{:S(2)}) copy-start(f32[3,256]{1,0:T(4,128)} %param.15) | copy-start | bytes 9220
  107.1 3.4 %copy-start.2 = (bf16[256,256]{1,0:T(8,128)(2,1)S(1)}, bf16[256,256]{1,0:T(8,128)(2,1)}, u32[]{:S(2)}) copy-start(bf16[256,256]{1,0:T(8,128)(2,1)} %param.12) | copy-start | bytes 393220
  107.2 47.0 %copy-start.6 = (f32[256,2]{0,1:T(2,128)S(1)}, f32[256,2]{0,1:T(2,128)}, u32[]{:S(2)}) copy-start(f32[256,2]{0,1:T(2,128)} %param.20) | copy-start | bytes 6148
  107.2 73.3 %reduce-scatter.3.cloned.1.call-start = ((), (), s32[]{:S(2)}) async-start(), calls=%async_computation.4 | async-start | bytes 1310720 | tf_op jit(solution)/shard_map/reduce_scatter | solution.py:47
  108.1 2.4 %collective-permute-start = (f32[2,256]{1,0:T(2,128)S(1)}, f32[2,256]{1,0:T(2,128)S(1)}, u32[]{:S(2)}, u32[]{:S(2)}) collective-permute-start(f32[2,256]{1,0:T(2,128)S(1)} %slice.34), channel_id=1, source_target_pairs={{0,4},{4,8},{8,12},{12,16},{16,20},{20,24},{24,28},{1,5},{5,9},{9,... | collective-permute-start | bytes 6152 | tf_op jit(solution)/shard_map/ppermute | solution.py:10
  149.0 24.1 %all-to-all-start.1 = ((bf16[8,1,86,512]{3,2,1,0:T(8,128)(2,1)}), bf16[8,1,86,512]{3,2,1,0:T(8,128)(2,1)S(1)}, u32[]{:S(2)}, u32[]{:S(2)}) async-start(bf16[8,1,86,512]{3,2,1,0:T(8,128)(2,1)} %bitcast.82), calls=%async_computation.3 | async-start | bytes 1441792 | tf_op jit(solution)/shard_map/all_to_all | solution.py:87
Sparse Core Ops, SparseCore 0:
  43.0 39.9 all-gather.1
  107.3 41.7 reduce-scatter.4
  152.5 27.9 reduce-scatter.2
where the time goes:
time: 187 us
  waiting for transfers between devices  98.8 us (53%)
  blocking collectives  25.7 us (14%)
  matrix products  23.7 us (13%)
  between operations  14 us (7%)
  local copies, waits for them, and re-layouts  10.9 us (6%)
  other arithmetic  7.69 us (4%)
  starting transfers between devices  6.31 us (3%)
    all_gather x1, waiting for transfers between devices, shards(): piece = lax.all_gather(arrived, 'tp', axis=1, tiled=True)  40 us
    reduce_scatter x1, waiting for transfers between devices, shards(): lax.psum_scatter(partial_out.astype(jnp.bfloat16), 'tp', scatter_dimensio...  37 us
    all_to_all x1, blocking collectives, shards(): lax.all_to_all(sent, 'ep', split_axis=0, concat_axis=0, tiled=True)  25.7 us
    all_to_all x1, waiting for transfers between devices, shards(): lax.all_to_all(summed, 'ep', split_axis=0, concat_axis=0, tiled=True)  18.8 us
    dot_general x1, matrix products, shards(): jnp.einsum('secf,efd->secd', hidden, down_proj, preferred_element_type=jn...  13 us
    dot_general x1, matrix products, shards(): jnp.einsum('secd,edf->secf', grouped_piece, up_proj, preferred_element_ty...  7.78 us
    all_to_all x1, starting transfers between devices, shards(): lax.all_to_all(summed, 'ep', split_axis=0, concat_axis=0, tiled=True)  4.61 us
  transfers between devices with their start and end apart: 5, of which 5 were waited for; matrix products, arithmetic and copies ran while one was open for 4% of the time, Pallas kernels for 0%

commit v1 on v0

--- a/solution.py
+++ b/solution.py
@@ -69,7 +69,8 @@
     )
     sent = jnp.dot(dispatch, own_columns, preferred_element_type=jnp.float32).astype(jnp.bfloat16)
     arrived = lax.all_to_all(sent, "ep", split_axis=0, concat_axis=0, tiled=True)
-    piece = lax.all_gather(arrived, "tp", axis=1, tiled=True)
+    try_all_the_teams = lambda xin: jnp.concatenate(lax.all_gather(xin, axis_name="tp"), axis=1)
+    piece = try_all_the_teams(arrived)
     grouped_piece = piece.reshape(ep_count, local_experts, capacity, piece.shape[1])
     gate_part = jnp.einsum(
         "secd,edf->secf", grouped_piece, gate_proj, preferred_element_type=jnp.float32

time: 187 us -> 195 us (1.043)
  local copies, waits for them, and re-layouts: 10.9 us -> 17.9 us
    reshape x0 -> x1, local copies, waits for them, and re-layouts: none -> 5.52 us  [shards(): jnp.concatenate(lax.all_gather(xin, axis_name='tp'), axis=1)]
where the time goes in v1:
time: 195 us; the launch traced here: 194 us
  waiting for transfers between devices  98.7 us (51%)
  blocking collectives  25.7 us (13%)
  matrix products  23.7 us (12%)
  local copies, waits for them, and re-layouts  17.9 us (9%)
  between operations  14 us (7%)
  other arithmetic  7.69 us (4%)
  starting transfers between devices  6.48 us (3%)
    all_gather x1, waiting for transfers between devices, shards(): lax.all_gather(xin, axis_name='tp')  40.2 us
    reduce_scatter x1, waiting for transfers between devices, shards(): lax.psum_scatter(partial_out.astype(jnp.bfloat16), 'tp', scatter_dimensio...  37 us
    all_to_all x1, blocking collectives, shards(): lax.all_to_all(sent, 'ep', split_axis=0, concat_axis=0, tiled=True)  25.7 us
    all_to_all x1, waiting for transfers between devices, shards(): lax.all_to_all(summed, 'ep', split_axis=0, concat_axis=0, tiled=True)  18.8 us
    dot_general x1, matrix products, shards(): jnp.einsum('secf,efd->secd', hidden, down_proj, preferred_element_type=jn...  13 us
    dot_general x1, matrix products, shards(): jnp.einsum('secd,edf->secf', grouped_piece, up_proj, preferred_element_ty...  7.78 us
    reshape x1, local copies, waits for them, and re-layouts, shards(): jnp.concatenate(lax.all_gather(xin, axis_name='tp'), axis=1)  5.52 us
    another operation x2, local copies, waits for them, and re-layouts  4.85 us
  transfers between devices with their start and end apart: 5, of which 5 were waited for; matrix products, arithmetic and copies ran while one was open for 4% of the time, Pallas kernels for 0%

profile of v1, /device:TPU:0, one launch (start us, length us, event | category | flops | bytes accessed | tf_op | source)
XLA Modules:
  0.0 194.2 jit_solution(4127801606866030137)
XLA Ops:
  7.2 0.0 copy-start
  7.2 0.0 copy-start.1
  7.2 0.0 all-gather.2.cloned.1.call-start
  7.2 0.9 copy.37
  8.2 0.1 eq.39
  8.3 0.1 reshape.114
  8.5 2.8 %convert_element_type.67 = f32[256,2048]{1,0:T(8,128)} convert(bf16[256,2048]{1,0:T(8,128)(2,1)} %param.17) | non-fusion elementwise | flops 524288 | bytes 3145728 | tf_op jit(solution)/shard_map/convert_element_type | solution.py:50
  11.3 0.3 multiply_reduce_fusion
  11.6 1.1 reduce-window.6
  12.8 0.2 slice_reduce_fusion
  13.0 0.1 fusion.41
  13.1 0.1 reduce_sum.51
  13.3 0.1 copy.39
  13.4 0.3 convert_reduce_fusion
  13.7 0.8 dynamic-slice
  14.4 1.5 convolution_convert_fusion.1
  15.9 0.2 all_to_all.9
  16.1 25.7 %all_to_all.14 = bf16[8,86,512]{2,1,0:T(8,128)(2,1)S(1)} all-to-all(bf16[8,86,512]{2,1,0:T(8,128)(2,1)S(1)} %all_to_all.9), channel_id=1, replica_groups=mesh['ep'=8,'tp'=4] {'ep'}, dimensions={0} | all-to-all | bytes 1409024 | tf_op jit(solution)/shard_map/all_to_all | solution.py:71
  41.8 1.1 all_gather.6
  42.9 0.0 all-gather.2.cloned.1.call-update
  42.9 0.0 reduce-scatter.5.cloned.1.call-start
  42.9 40.2 %all-gather.2.cloned.1.call-done = bf16[4,688,512]{2,1,0:T(8,128)(2,1)} async-done(((bf16[1,688,512]{2,1,0:T(8,128)(2,1)}), bf16[4,688,512]{2,1,0:T(8,128)(2,1)}) %all-gather.2.cloned.1.call-update) | async-done | bytes 2818064 | tf_op jit(solution)/shard_map/all_gather | solution.py:72
  83.1 5.5 %copy.41 = bf16[688,4,512]{2,1,0:T(4,128)(2,1)} copy(bf16[688,4,512]{2,0,1:T(8,128)(2,1)} %bitcast.83) | data formatting | bytes 5636096 | tf_op jit(solution)/shard_map/reshape | solution.py:72
  88.6 4.8 %reshape.117 = bf16[8,86,2048]{2,1,0:T(8,128)(2,1)} reshape(bf16[688,4,512]{2,1,0:T(4,128)(2,1)} %copy.41) | data formatting | bytes 5636096 | tf_op jit(solution)/shard_map/reshape.9
  93.5 7.8 %fusion.2 = f32[8,86,1024]{2,1,0:T(8,128)} fusion(bf16[8,86,2048]{2,1,0:T(8,128)(2,1)} %reshape.117, bf16[1,2048,1024]{2,1,0:T(8,128)(2,1)} %param.22), kind=kOutput, calls=%fused_computation.3 | convolution fusion | flops 2885681152 | bytes 9830400 | tf_op jit(solution)/shard_map/secd,edf->secf/dot_general | solution.py:78
  101.2 13.0 %fusion.9 = bf16[8,1,86,2048]{3,2,0,1:T(8,128)(2,1)} fusion(bf16[1,1024,2048]{2,1,0:T(8,128)(2,1)} %param.23, f32[8,86,1024]{2,1,0:T(8,128)} %fusion.2, bf16[8,86,2048]{2,1,0:T(8,128)(2,1)} %reshape.117, bf16[1,2048,1024]{2,1,0:T(8,128)(2,1)} %param.21), kind=kOutput, calls=%fused_computation.8 | convolution fusion | flops 5776998400 | bytes 16842752 | tf_op jit(solution)/shard_map/secf,efd->secd/dot_general | solution.py:82
  114.3 0.0 reduce-scatter.5.cloned.1.call-update
  114.3 0.0 copy-start.6
  114.3 0.0 reduce-scatter.3.cloned.1.call-start
  114.4 0.8 copy-done.3
  115.2 0.1 copy-done.4
  115.3 1.8 collective-permute-start
  117.1 0.6 collective-permute-done
  117.7 0.0 copy-done.2
  117.7 1.4 convolution_convert_fusion
  119.1 0.0 reduce-scatter.3.cloned.1.call-update
  119.2 37.0 %reduce-scatter.5.cloned.1.call-done = bf16[8,1,86,512]{3,2,0,1:T(8,128)(2,1)} async-done(((bf16[8,1,86,2048]{3,2,0,1:T(8,128)(2,1)}), bf16[8,1,86,512]{3,2,0,1:T(8,128)(2,1)}) %reduce-scatter.5.cloned.1.call-update) | async-done | bytes 704528 | tf_op jit(solution)/shard_map/reduce_scatter | solution.py:85
  156.2 4.6 %all-to-all-start.1 = ((bf16[8,1,86,512]{3,2,1,0:T(8,128)(2,1)}), bf16[8,1,86,512]{3,2,1,0:T(8,128)(2,1)S(1)}, u32[]{:S(2)}, u32[]{:S(2)}) async-start(bf16[8,1,86,512]{3,2,1,0:T(8,128)(2,1)} %bitcast.84), calls=%async_computation.3 | async-start | bytes 1441792 | tf_op jit(solution)/shard_map/all_to_all | solution.py:88
  160.8 0.1 copy.43
  161.0 0.1 mul.120
  161.1 0.2 copy.40
  161.3 0.1 copy.36
  161.5 18.8 %all-to-all-done.1 = bf16[8,1,86,512]{3,2,1,0:T(8,128)(2,1)S(1)} async-done(((bf16[8,1,86,512]{3,2,1,0:T(8,128)(2,1)}), bf16[8,1,86,512]{3,2,1,0:T(8,128)(2,1)S(1)}, u32[]{:S(2)}, u32[]{:S(2)}) %all-to-all-start.1) | async-done | bytes 704544 | tf_op jit(solution)/shard_map/all_to_all | solution.py:88
  180.3 0.2 reshape.122
  180.5 2.0 %gather_fusion = bf16[512,512]{1,0:T(8,128)(2,1)S(1)} fusion(bf16[688,512]{1,0:T(8,128)(2,1)S(1)} %reshape.122, s32[1024]{0:T(1024)S(1)} %pad_clamp_fusion), kind=kCustom, calls=%fused_computation | custom fusion | bytes 1050624 | tf_op jit(solution)/shard_map/jit(_take)/gather | solution.py:90
  182.5 0.2 gather.7
  182.7 2.9 %multiply_reduce_fusion.1 = bf16[256,512]{1,0:T(8,128)(2,1)} fusion(bf16[256,2,512]{2,1,0:T(2,128)(2,1)S(1)} %gather.7, pred[256,2]{1,0:T(8,128)(4,1)S(1)} %copy.40, f32[256,2]{1,0:T(8,128)S(1)} %copy.36), kind=kLoop, calls=%fused_computation.22 | loop fusion | flops 917504 | bytes 788992 | tf_op jit(solution)/shard_map/reduce_sum | solution.py:94
  185.6 2.0 %reduce-scatter.3.cloned.1.call-done = bf16[256,512]{1,0:T(8,128)(2,1)} async-done(((bf16[256,2048]{1,0:T(8,128)(2,1)}), bf16[256,512]{1,0:T(8,128)(2,1)}) %reduce-scatter.3.cloned.1.call-update) | async-done | bytes 262160 | tf_op jit(solution)/shard_map/reduce_scatter | solution.py:47
  (23 shorter events, 0.2 us)
Async XLA Ops:
  7.2 110.5 %copy-start = (bf16[256,2048]{1,0:T(8,128)(2,1)S(1)}, bf16[256,2048]{1,0:T(8,128)(2,1)}, u32[]{:S(2)}) copy-start(bf16[256,2048]{1,0:T(8,128)(2,1)} %param.16) | copy-start | bytes 3145732
  7.2 6.2 %copy-start.5 = (s32[256,2]{0,1:T(2,128)S(1)}, s32[256,2]{0,1:T(2,128)}, u32[]{:S(2)}) copy-start(s32[256,2]{0,1:T(2,128)} %param.19) | copy-start | bytes 6148
  7.2 4.1 %copy-start.1 = (bf16[256,2048]{1,0:T(8,128)(2,1)S(1)}, bf16[256,2048]{1,0:T(8,128)(2,1)}, u32[]{:S(2)}) copy-start(bf16[256,2048]{1,0:T(8,128)(2,1)} %param.17) | copy-start | bytes 3145732
  7.2 75.9 %all-gather.2.cloned.1.call-start = ((), (), s32[]{:S(2)}) async-start(), calls=%async_computation.5 | async-start | bytes 3522560 | tf_op jit(solution)/shard_map/all_gather | solution.py:72
  42.9 113.3 %reduce-scatter.5.cloned.1.call-start = ((), (), s32[]{:S(2)}) async-start(), calls=%async_computation.6 | async-start | bytes 3604480 | tf_op jit(solution)/shard_map/reduce_scatter | solution.py:85
  114.3 0.9 copy-start.3
  114.3 1.0 copy-start.4
  114.3 2.8 %copy-start.7 = (f32[3,256]{1,0:T(4,128)S(1)}, f32[3,256]{1,0:T(4,128)}, u32[]{:S(2)}) copy-start(f32[3,256]{1,0:T(4,128)} %param.15) | copy-start | bytes 9220
  114.3 3.4 %copy-start.2 = (bf16[256,256]{1,0:T(8,128)(2,1)S(1)}, bf16[256,256]{1,0:T(8,128)(2,1)}, u32[]{:S(2)}) copy-start(bf16[256,256]{1,0:T(8,128)(2,1)} %param.12) | copy-start | bytes 393220
  114.3 47.0 %copy-start.6 = (f32[256,2]{0,1:T(2,128)S(1)}, f32[256,2]{0,1:T(2,128)}, u32[]{:S(2)}) copy-start(f32[256,2]{0,1:T(2,128)} %param.20) | copy-start | bytes 6148
  114.3 73.3 %reduce-scatter.3.cloned.1.call-start = ((), (), s32[]{:S(2)}) async-start(), calls=%async_computation.4 | async-start | bytes 1310720 | tf_op jit(solution)/shard_map/reduce_scatter | solution.py:47
  115.3 2.4 %collective-permute-start = (f32[2,256]{1,0:T(2,128)S(1)}, f32[2,256]{1,0:T(2,128)S(1)}, u32[]{:S(2)}, u32[]{:S(2)}) collective-permute-start(f32[2,256]{1,0:T(2,128)S(1)} %slice.34), channel_id=1, source_target_pairs={{0,4},{4,8},{8,12},{12,16},{16,20},{20,24},{24,28},{1,5},{5,9},{9,... | collective-permute-start | bytes 6152 | tf_op jit(solution)/shard_map/ppermute | solution.py:10
  156.2 24.1 %all-to-all-start.1 = ((bf16[8,1,86,512]{3,2,1,0:T(8,128)(2,1)}), bf16[8,1,86,512]{3,2,1,0:T(8,128)(2,1)S(1)}, u32[]{:S(2)}, u32[]{:S(2)}) async-start(bf16[8,1,86,512]{3,2,1,0:T(8,128)(2,1)} %bitcast.84), calls=%async_computation.3 | async-start | bytes 1441792 | tf_op jit(solution)/shard_map/all_to_all | solution.py:88
Sparse Core Ops, SparseCore 0:
  43.0 40.0 all-gather.1
  114.4 41.7 reduce-scatter.4
  159.7 27.9 reduce-scatter.2
